TPU v7x, 32 devices: a whole 2x2x4 slice. The times are simulated.
32 devices in a mesh: grp: 2 (over y), sp: 4 (over z), dp: 4 (over x, core).
Axes of the slice: x: 2, y: 2, z: 4, core: 2. Of those that a mesh axis runs over, the one named last changes fastest.
Arguments:
- gate_input: bfloat16 [8, 1536, 2048], P(('grp', 'dp'), 'sp'), parts along dimension 0, may hold values from -6 to 6
- value_input: bfloat16 [8, 1536, 2048], P(('grp', 'dp'), 'sp'), parts along dimension 0, may hold values from -6 to 6
- norm_gain: bfloat16 [2048], replicated, may hold values from 0.099609375 to 1.8984375
- norm_bias: bfloat16 [2048], replicated, may hold values from -2.5 to 2.5
- mix_weight: bfloat16 [16, 1024, 1024], P('sp', 'dp'), may hold values from -0.1875 to 0.1875
- mix_bias: bfloat16 [16, 1024], P('sp'), may hold values from 0.099609375 to 1.8984375
Outputs:
- gated: bfloat16 [8, 1536, 2048], P(('grp', 'dp'), 'sp'), parts along dimension 0
There are 2 independent parts, one for each index of `grp`. A program takes and returns all parts, laid end to end along the dimension named above; an argument that names none is the same for every part. Nothing has to cross between parts.
All inputs are finite; a program needn't handle non-finite values.
Results may differ from a plain program's by a relative error of at most 0.0053.
Values may be sent and summed in bfloat16 or wider, within the bound.
A program may use at most 64 MiB of HBM per device.

v0:
```python
import jax
import jax.numpy as jnp
from jax import lax
from jax.sharding import PartitionSpec as P

GD = 128
BLK = 1024


def mix_groups(normed_ex, mix_weight, mix_bias):
    seqs, length, local_width = normed_ex.shape
    groups_here = mix_weight.shape[0]
    nblocks = -(-length // BLK)
    padded = jnp.pad(normed_ex, ((0, 0), (0, nblocks * BLK - length), (0, 0)))
    blocks = padded.reshape(seqs * nblocks, BLK, groups_here, GD)
    piece = lax.all_gather(mix_weight, "dp", axis=1, tiled=True)
    count = piece.shape[1]
    rows = lax.iota(jnp.int32, count)
    cols = lax.iota(jnp.int32, BLK)
    keep = cols[None, :] <= rows[:, None]
    masked = jnp.where(keep[None], piece, jnp.zeros_like(piece))
    term = jnp.einsum("gts,bsgc->btgc", masked, blocks, preferred_element_type=jnp.float32)
    bias_rows = mix_bias.astype(jnp.float32)
    mixed = term + bias_rows.T[None, :, :, None]
    mixed = mixed.reshape(seqs, nblocks * BLK, local_width)[:, :length]
    return mixed.astype(jnp.bfloat16)


def body(gate_input, value_input, norm_gain, norm_bias, mix_weight, mix_bias):
    act = jax.nn.gelu(value_input.astype(jnp.float32))
    mean = jnp.mean(act, axis=-1, keepdims=True)
    var = jnp.mean(jnp.square(act - mean), axis=-1, keepdims=True)
    normed = (
        (act - mean) * lax.rsqrt(var + 1e-06) * norm_gain.astype(jnp.float32)
        + norm_bias.astype(jnp.float32)
    ).astype(jnp.bfloat16)
    normed_ex = lax.all_to_all(normed, "sp", split_axis=2, concat_axis=1, tiled=True)
    mixed = mix_groups(normed_ex, mix_weight, mix_bias)
    returned = lax.all_to_all(mixed, "sp", split_axis=1, concat_axis=2, tiled=True)
    gated = jax.nn.gelu(gate_input.astype(jnp.float32)) * returned.astype(jnp.float32)
    return gated.astype(jnp.bfloat16)


def solution(mesh):
    placed = (
        P(("grp", "dp"), "sp", None),
        P(("grp", "dp"), "sp", None),
        P(),
        P(),
        P("sp", "dp", None),
        P("sp", None),
    )
    return jax.shard_map(
        body, mesh=mesh, in_specs=placed, out_specs=P(("grp", "dp"), "sp", None), check_vma=False
    )
```

profile of v0, /device:TPU:0, one launch (start us, length us, event | category | flops | bytes accessed | tf_op | source)
XLA Modules:
  0.0 239.9 jit_solution(9603832664579578522)
XLA Ops:
  6.5 0.0 copy-start
  6.5 0.0 copy-start.4
  6.5 0.0 copy-start.5
  6.5 0.0 all-gather.2.cloned.1.call-start
  6.5 0.7 all-gather.2.cloned.1.call-update
  7.3 0.7 copy-done
  7.9 0.9 copy.17
  8.8 0.0 copy-done.4
  8.8 0.0 copy-done.5
  8.8 1.1 fusion.23
  10.0 1.3 multiply_reduce_fusion
  11.3 1.5 add_convert_fusion
  12.9 30.1 %copy.35 = bf16[1,384,2048]{1,0,2:T(2,128)(2,1)S(1)} copy(bf16[1,384,2048]{1,2,0:T(8,128)(2,1)S(1)} %add_convert_fusion) | data formatting | bytes 3145728 | tf_op jit(solution)/shard_map/convert_element_type | solution.py:36
  43.0 0.5 broadcast.85
  43.5 34.4 %reduce.2 = bf16[2048,384]{1,0:T(8,128)(2,1)} reduce(bf16[2048,1,384]{2,1,0:T(2,128)(2,1)S(1)} %bitcast.31, bf16[]{:T(256)} %broadcast.85), dimensions={1}, to_apply=%bitcast.30.reduce_sub_computation | reduce | bytes 3145730
  77.9 0.0 copy-start.3
  77.9 3.7 %reshape.69 = bf16[4,2,98304]{2,1,0:T(2,128)(2,1)} reshape(bf16[2048,384]{1,0:T(8,128)(2,1)} %reduce.2) | data formatting | bytes 3145728
  81.7 6.3 %all-to-all-start = ((bf16[4,2,98304]{2,1,0:T(2,128)(2,1)}), bf16[4,2,98304]{2,1,0:T(2,128)(2,1)}, u32[]{:S(2)}, u32[]{:S(2)}) async-start(bf16[4,2,98304]{2,1,0:T(2,128)(2,1)} %reshape.69), calls=%async_computation | async-start | bytes 3145728 | tf_op jit(solution)/shard_map/all_to_all | solution.py:37
  88.0 1.3 iota_compare_fusion
  89.3 0.0 copy-done.3
  89.3 35.8 %all-to-all-done = bf16[4,2,98304]{2,1,0:T(2,128)(2,1)} async-done(((bf16[4,2,98304]{2,1,0:T(2,128)(2,1)}), bf16[4,2,98304]{2,1,0:T(2,128)(2,1)}, u32[]{:S(2)}, u32[]{:S(2)}) %all-to-all-start) | async-done | bytes 1572896 | tf_op jit(solution)/shard_map/all_to_all | solution.py:37
  125.1 3.1 %reshape.70 = bf16[2048,1,384]{2,1,0:T(2,128)(2,1)S(1)} reshape(bf16[4,2,98304]{2,1,0:T(2,128)(2,1)} %all-to-all-done) | data formatting | bytes 3145728
  128.2 1.4 copy.27
  129.6 2.6 %copy.19 = bf16[1,4,384,512]{3,2,1,0:T(8,128)(2,1)} copy(bf16[1,4,384,512]{2,3,1,0:T(8,128)(2,1)} %bitcast.36) | data formatting | bytes 3145728 | tf_op jit(solution)/shard_map/all_to_all | solution.py:37
  132.2 0.0 copy-start.2
  132.2 1.6 pad.4
  133.8 2.1 reshape.64
  135.9 0.0 all-gather.2.cloned.1.call-done
  135.9 0.0 copy-done.2
  135.9 8.1 %fusion.4 = bf16[2,1024,4,128]{1,3,0,2:T(8,128)(2,1)} fusion(f32[1024,4]{0,1:T(4,128)S(1)} %convert_bitcast_fusion.1, bf16[4,1024,1024]{2,1,0:T(8,128)(2,1)} %all-gather.2.cloned.1.call-done, pred[1024,1024]{1,0:T(8,128)(4,1)S(1)} %copy-done.2, bf16[2,1024,4,128]{3,2,1,0:T(4,128)(2,1)} %reshape.64), kind=kOutput, calls=%fused_computation.13 | convolution fusion | flops 2153775104 | bytes 13647872 | tf_op jit(solution)/shard_map/gts,bsgc->btgc/dot_general | solution.py:22
  144.0 3.1 %copy.21 = bf16[2,1024,4,128]{3,2,1,0:T(4,128)(2,1)S(1)} copy(bf16[2,1024,4,128]{1,3,0,2:T(8,128)(2,1)} %fusion.4) | data formatting | bytes 4194304 | tf_op jit(solution)/shard_map/convert.5
  147.2 2.2 reshape.65
  149.4 0.0 slice-start
  149.4 1.4 slice-done
  150.8 11.7 %copy.34 = bf16[1,1536,512]{2,0,1:T(2,128)(2,1)S(1)} copy(bf16[1,1536,512]{2,1,0:T(8,128)(2,1)S(1)} %slice-done) | data formatting | bytes 3145728 | tf_op jit(solution)/shard_map/slice | solution.py:25
  162.5 11.1 %reduce.3 = bf16[1536,512]{1,0:T(8,128)(2,1)} reduce(bf16[1536,1,512]{2,1,0:T(2,128)(2,1)S(1)} %bitcast.32, bf16[]{:T(256)} %broadcast.85), dimensions={1}, to_apply=%bitcast.29.reduce_sub_computation | reduce | bytes 3145730
  173.5 0.0 copy-start.1
  173.5 4.3 %reshape.71 = bf16[4,2,98304]{2,1,0:T(2,128)(2,1)} reshape(bf16[1536,512]{1,0:T(8,128)(2,1)} %reduce.3) | data formatting | bytes 3145728
  177.8 4.3 %all-to-all-start.1 = ((bf16[4,2,98304]{2,1,0:T(2,128)(2,1)}), bf16[4,2,98304]{2,1,0:T(2,128)(2,1)}, u32[]{:S(2)}, u32[]{:S(2)}) async-start(bf16[4,2,98304]{2,1,0:T(2,128)(2,1)} %reshape.71), calls=%async_computation.1 | async-start | bytes 3145728 | tf_op jit(solution)/shard_map/all_to_all | solution.py:39
  182.1 0.0 copy-done.1
  182.2 1.6 copy.16
  183.7 35.0 %all-to-all-done.1 = bf16[4,2,98304]{2,1,0:T(2,128)(2,1)} async-done(((bf16[4,2,98304]{2,1,0:T(2,128)(2,1)}), bf16[4,2,98304]{2,1,0:T(2,128)(2,1)}, u32[]{:S(2)}, u32[]{:S(2)}) %all-to-all-start.1) | async-done | bytes 1572896 | tf_op jit(solution)/shard_map/all_to_all | solution.py:39
  218.7 3.1 %reshape.72 = bf16[1536,1,512]{2,1,0:T(2,128)(2,1)S(1)} reshape(bf16[4,2,98304]{2,1,0:T(2,128)(2,1)} %all-to-all-done.1) | data formatting | bytes 3145728
  221.8 0.4 copy.23
  222.2 2.1 convert_bitcast_fusion
  224.3 2.4 copy.24
  226.7 3.8 %fusion.12 = bf16[1,384,2048]{1,2,0:T(8,128)(2,1)} fusion(bf16[1,384,2048]{1,2,0:T(8,128)(2,1)} %copy.16, f32[1,384,4,512]{1,3,2,0:T(8,128)S(1)} %copy.24), kind=kLoop, calls=%fused_computation.22 | loop fusion | flops 8650752 | bytes 6291456 | tf_op jit(solution)/shard_map/convert_element_type | solution.py:41
  230.5 2.6 %copy.25 = bf16[1,384,2048]{2,1,0:T(8,128)(2,1)} copy(bf16[1,384,2048]{1,2,0:T(8,128)(2,1)} %fusion.12) | data formatting | bytes 3145728 | tf_op jit(solution)/shard_map/convert_element_type | solution.py:41
  (5 shorter events, 0.0 us)
Async XLA Ops:
  6.5 1.4 copy-start
  6.5 2.3 copy-start.4
  6.5 2.3 copy-start.5
  6.5 129.4 %all-gather.2.cloned.1.call-start = ((), (), s32[]{:S(2)}) async-start(), calls=%async_computation.2 | async-start | bytes 10485760 | tf_op jit(solution)/shard_map/all_gather | solution.py:16
  77.9 11.4 %copy-start.3 = (bf16[4,1024]{1,0:T(4,128)(2,1)S(1)}, bf16[4,1024]{1,0:T(4,128)(2,1)}, u32[]{:S(2)}) copy-start(bf16[4,1024]{1,0:T(4,128)(2,1)} %param.11) | copy-start | bytes 24580
  81.7 43.4 %all-to-all-start = ((bf16[4,2,98304]{2,1,0:T(2,128)(2,1)}), bf16[4,2,98304]{2,1,0:T(2,128)(2,1)}, u32[]{:S(2)}, u32[]{:S(2)}) async-start(bf16[4,2,98304]{2,1,0:T(2,128)(2,1)} %reshape.69), calls=%async_computation | async-start | bytes 3145728 | tf_op jit(solution)/shard_map/all_to_all | solution.py:37
  132.2 3.7 %copy-start.2 = (pred[1024,1024]{1,0:T(8,128)(4,1)S(1)}, pred[1024,1024]{1,0:T(8,128)(4,1)}, u32[]{:S(2)}) copy-start(pred[1024,1024]{1,0:T(8,128)(4,1)} %iota_compare_fusion) | copy-start | bytes 3145732
  149.4 1.4 slice-start
  173.5 8.6 %copy-start.1 = (bf16[1,384,2048]{2,1,0:T(8,128)(2,1)S(1)}, bf16[1,384,2048]{2,1,0:T(8,128)(2,1)}, u32[]{:S(2)}) copy-start(bf16[1,384,2048]{2,1,0:T(8,128)(2,1)} %param.6) | copy-start | bytes 4718596
  177.8 40.9 %all-to-all-start.1 = ((bf16[4,2,98304]{2,1,0:T(2,128)(2,1)}), bf16[4,2,98304]{2,1,0:T(2,128)(2,1)}, u32[]{:S(2)}, u32[]{:S(2)}) async-start(bf16[4,2,98304]{2,1,0:T(2,128)(2,1)} %reshape.71), calls=%async_computation.1 | async-start | bytes 3145728 | tf_op jit(solution)/shard_map/all_to_all | solution.py:39
Sparse Core Ops, SparseCore 0:
  8.9 60.9 all-gather.1
where the time goes:
time: 241 us; the launch traced here: 240 us
  local copies, waits for them, and re-layouts  79.4 us (33%)
  waiting for transfers between devices  71.5 us (30%)
  other arithmetic  56.7 us (24%)
  between operations  13.5 us (6%)
  starting transfers between devices  10.7 us (4%)
  matrix products  8.09 us (3%)
    unnamed x2, other arithmetic  45.5 us
    all_to_all x1, waiting for transfers between devices, body(): lax.all_to_all(normed, 'sp', split_axis=2, concat_axis=1, tiled=True)  35.8 us
    all_to_all x1, waiting for transfers between devices, body(): lax.all_to_all(mixed, 'sp', split_axis=1, concat_axis=2, tiled=True)  35 us
    convert_element_type x1, local copies, waits for them, and re-layouts, body(): normed = ((act - mean) * lax.rsqrt(var + 1e-06) * norm_gain.astype(jnp.fl...  30.1 us
    unnamed x20, local copies, waits for them, and re-layouts  19.2 us
    slice x3, local copies, waits for them, and re-layouts, mix_groups(): mixed = mixed.reshape(seqs, nblocks * BLK, local_width)[:, :length]  13.1 us
    dot_general x1, matrix products, mix_groups(): jnp.einsum('gts,bsgc->btgc', masked, blocks, preferred_element_type=jnp.f...  8.09 us
    all_to_all x1, starting transfers between devices, body(): lax.all_to_all(normed, 'sp', split_axis=2, concat_axis=1, tiled=True)  6.35 us
  transfers between devices with their start and end apart: 3, of which 2 were waited for; matrix products, arithmetic and copies ran while one was open for 36% of the time, Pallas kernels for 0%

commit v1 on v0

--- a/solution.py
+++ b/solution.py
@@ -34,7 +34,10 @@
         (act - mean) * lax.rsqrt(var + 1e-06) * norm_gain.astype(jnp.float32)
         + norm_bias.astype(jnp.float32)
     ).astype(jnp.bfloat16)
-    normed_ex = lax.all_to_all(normed, "sp", split_axis=2, concat_axis=1, tiled=True)
+    normed_ex = jnp.concatenate(
+        lax.all_to_all(jnp.stack(jnp.split(normed, lax.axis_size("sp"), axis=2)), "sp", 0, 0),
+        axis=1,
+    )
     mixed = mix_groups(normed_ex, mix_weight, mix_bias)
     returned = lax.all_to_all(mixed, "sp", split_axis=1, concat_axis=2, tiled=True)
     gated = jax.nn.gelu(gate_input.astype(jnp.float32)) * returned.astype(jnp.float32)

time: 241 us -> 176 us (0.73)
  local copies, waits for them, and re-layouts: 79.4 us -> 41.3 us
  other arithmetic: 56.7 us -> 21.5 us
  waiting for transfers between devices: 71.5 us -> 80.1 us
    unnamed x2 -> x1, other arithmetic: 45.5 us -> 11 us
    convert_element_type x1 -> x0, local copies, waits for them, and re-layouts: 30.1 us -> none  [body(): normed = ((act - mean) * lax.rsqrt(var + 1e-06) * norm_gain.astype(jnp.fl...]
    unnamed x20 -> x17, local copies, waits for them, and re-layouts: 19.2 us -> 12.1 us
    all_gather x1, waiting for transfers between devices: 0.01 us -> 6.87 us  [mix_groups(): piece = lax.all_gather(mix_weight, 'dp', axis=1, tiled=True)]
    all_to_all x1 -> x0, local copies, waits for them, and re-layouts: 2.64 us -> none  [body(): lax.all_to_all(normed, 'sp', split_axis=2, concat_axis=1, tiled=True)]
    another operation x1 -> x3, local copies, waits for them, and re-layouts: 3.13 us -> 4.92 us
  transfers between devices with their start and end apart: 3 -> 3, of which waited for: 2 -> 3; matrix products, arithmetic and copies ran while one was open for 36% -> 7% of each run, Pallas kernels for 0% -> 0%
where the time goes in v1:
time: 176 us; the launch traced here: 175 us
  waiting for transfers between devices  80.1 us (46%)
  local copies, waits for them, and re-layouts  41.3 us (23%)
  other arithmetic  21.5 us (12%)
  between operations  13.5 us (8%)
  starting transfers between devices  10.9 us (6%)
  matrix products  8.1 us (5%)
    all_to_all x1, waiting for transfers between devices, body(): lax.all_to_all(jnp.stack(jnp.split(normed, lax.axis_size('sp'), axis=2)),...  36.6 us
    all_to_all x1, waiting for transfers between devices, body(): lax.all_to_all(mixed, 'sp', split_axis=1, concat_axis=2, tiled=True)  35.9 us
    slice x3, local copies, waits for them, and re-layouts, mix_groups(): mixed = mixed.reshape(seqs, nblocks * BLK, local_width)[:, :length]  13.1 us
    unnamed x17, local copies, waits for them, and re-layouts  12.1 us
    unnamed x1, other arithmetic  11 us
    dot_general x1, matrix products, mix_groups(): jnp.einsum('gts,bsgc->btgc', masked, blocks, preferred_element_type=jnp.f...  8.1 us
    all_gather x1, waiting for transfers between devices, mix_groups(): piece = lax.all_gather(mix_weight, 'dp', axis=1, tiled=True)  6.87 us
    all_to_all x1, starting transfers between devices, body(): lax.all_to_all(jnp.stack(jnp.split(normed, lax.axis_size('sp'), axis=2)),...  6.35 us
  transfers between devices with their start and end apart: 3, of which 3 were waited for; matrix products, arithmetic and copies ran while one was open for 7% of the time, Pallas kernels for 0%

profile of v1, /device:TPU:0, one launch (start us, length us, event | category | flops | bytes accessed | tf_op | source)
XLA Modules:
  0.0 175.5 jit_solution(3552523051469836391)
XLA Ops:
  6.5 0.0 copy-start.1
  6.5 0.0 copy-start.4
  6.5 0.0 copy-start.5
  6.5 0.0 all-gather.2.cloned.1.call-start
  6.5 0.7 all-gather.2.cloned.1.call-update
  7.3 0.7 copy-done.1
  7.9 0.9 copy.23
  8.8 0.0 copy-done.4
  8.8 0.0 copy-done.5
  8.8 1.1 fusion.23
  10.0 1.3 multiply_reduce_fusion
  11.3 1.5 add_convert_fusion
  12.9 0.2 slice_bitcast_fusion.3
  13.1 0.2 pad_maximum_fusion
  13.3 0.0 copy-start.3
  13.3 1.6 copy.24
  15.0 6.3 %all-to-all-start = ((bf16[4,1,384,512]{3,2,1,0:T(8,128)(2,1)}), bf16[4,1,384,512]{3,2,1,0:T(8,128)(2,1)S(1)}, u32[]{:S(2)}, u32[]{:S(2)}) async-start(bf16[4,1,384,512]{3,2,1,0:T(8,128)(2,1)} %copy.24), calls=%async_computation | async-start | bytes 3145728 | tf_op jit(solution)/shard_map/all_to_all | solution.py:38
  21.3 0.3 iota_compare_fusion
  21.6 0.0 copy-done.3
  21.6 36.6 %all-to-all-done = bf16[4,1,384,512]{3,2,1,0:T(8,128)(2,1)S(1)} async-done(((bf16[4,1,384,512]{3,2,1,0:T(8,128)(2,1)}), bf16[4,1,384,512]{3,2,1,0:T(8,128)(2,1)S(1)}, u32[]{:S(2)}, u32[]{:S(2)}) %all-to-all-start) | async-done | bytes 1572896 | tf_op jit(solution)/shard_map/all_to_all | solution.py:38
  58.3 0.0 copy-start
  58.3 1.1 copy-done
  59.4 1.5 pad.4
  61.0 2.1 %reshape.68 = bf16[2,1024,4,128]{3,2,1,0:T(4,128)(2,1)} reshape(bf16[1,2048,512]{2,1,0:T(8,128)(2,1)S(1)} %pad.4) | data formatting | bytes 4194304 | tf_op jit(solution)/shard_map/reshape | solution.py:15
  63.0 6.9 %all-gather.2.cloned.1.call-done = bf16[4,1024,1024]{2,1,0:T(8,128)(2,1)} async-done(((bf16[4,256,1024]{2,1,0:T(8,128)(2,1)}), bf16[4,1024,1024]{2,1,0:T(8,128)(2,1)}) %all-gather.2.cloned.1.call-update) | async-done | bytes 8388624 | tf_op jit(solution)/shard_map/all_gather | solution.py:16
  69.9 8.1 %fusion.4 = bf16[2,1024,4,128]{1,3,0,2:T(8,128)(2,1)} fusion(f32[1024,4]{0,1:T(4,128)S(1)} %convert_bitcast_fusion.1, bf16[4,1024,1024]{2,1,0:T(8,128)(2,1)} %all-gather.2.cloned.1.call-done, pred[1024,1024]{1,0:T(8,128)(4,1)S(1)} %iota_compare_fusion, bf16[2,1024,4,128]{3,2,1,0:T(4,128)(2,1)} %reshape.68), kind=kOutput, calls=%fused_computation.13 | convolution fusion | flops 2153775104 | bytes 13647872 | tf_op jit(solution)/shard_map/gts,bsgc->btgc/dot_general | solution.py:22
  78.0 3.1 %copy.26 = bf16[2,1024,4,128]{3,2,1,0:T(4,128)(2,1)S(1)} copy(bf16[2,1024,4,128]{1,3,0,2:T(8,128)(2,1)} %fusion.4) | data formatting | bytes 4194304 | tf_op jit(solution)/shard_map/convert.5
  81.2 2.2 %reshape.69 = bf16[1,2048,512]{2,1,0:T(8,128)(2,1)} reshape(bf16[2,1024,4,128]{3,2,1,0:T(4,128)(2,1)S(1)} %copy.26) | data formatting | bytes 4194304 | tf_op jit(solution)/shard_map/reshape | solution.py:25
  83.4 0.0 slice-start
  83.4 1.4 slice-done
  84.8 11.7 %copy.37 = bf16[1,1536,512]{2,0,1:T(2,128)(2,1)S(1)} copy(bf16[1,1536,512]{2,1,0:T(8,128)(2,1)S(1)} %slice-done) | data formatting | bytes 3145728 | tf_op jit(solution)/shard_map/slice | solution.py:25
  96.5 0.5 broadcast.85
  97.0 11.0 %reduce.2 = bf16[1536,512]{1,0:T(8,128)(2,1)} reduce(bf16[1536,1,512]{2,1,0:T(2,128)(2,1)S(1)} %bitcast.32, bf16[]{:T(256)} %broadcast.85), dimensions={1}, to_apply=%bitcast.31.reduce_sub_computation | reduce | bytes 3145730
  108.0 0.0 copy-start.2
  108.0 4.2 %reshape.73 = bf16[4,2,98304]{2,1,0:T(2,128)(2,1)} reshape(bf16[1536,512]{1,0:T(8,128)(2,1)} %reduce.2) | data formatting | bytes 3145728
  112.2 4.6 %all-to-all-start.1 = ((bf16[4,2,98304]{2,1,0:T(2,128)(2,1)}), bf16[4,2,98304]{2,1,0:T(2,128)(2,1)}, u32[]{:S(2)}, u32[]{:S(2)}) async-start(bf16[4,2,98304]{2,1,0:T(2,128)(2,1)} %reshape.73), calls=%async_computation.1 | async-start | bytes 3145728 | tf_op jit(solution)/shard_map/all_to_all | solution.py:42
  116.8 0.0 copy-done.2
  116.8 1.6 copy.22
  118.4 35.9 %all-to-all-done.1 = bf16[4,2,98304]{2,1,0:T(2,128)(2,1)} async-done(((bf16[4,2,98304]{2,1,0:T(2,128)(2,1)}), bf16[4,2,98304]{2,1,0:T(2,128)(2,1)}, u32[]{:S(2)}, u32[]{:S(2)}) %all-to-all-start.1) | async-done | bytes 1572896 | tf_op jit(solution)/shard_map/all_to_all | solution.py:42
  154.3 3.1 %reshape.74 = bf16[1536,1,512]{2,1,0:T(2,128)(2,1)S(1)} reshape(bf16[4,2,98304]{2,1,0:T(2,128)(2,1)} %all-to-all-done.1) | data formatting | bytes 3145728
  157.4 0.4 copy.28
  157.8 2.1 %convert_bitcast_fusion = f32[1,384,4,512]{3,1,2,0:T(8,128)} fusion(bf16[1,4,384,512]{3,2,1,0:T(8,128)(2,1)S(1)} %bitcast.35), kind=kLoop, calls=%fused_computation.28 | loop fusion | flops 786432 | bytes 4718592 | tf_op jit(solution)/shard_map/convert_element_type | solution.py:43
  159.9 2.4 %copy.29 = f32[1,384,4,512]{1,3,2,0:T(8,128)S(1)} copy(f32[1,384,4,512]{3,1,2,0:T(8,128)} %convert_bitcast_fusion) | data formatting | bytes 6291456 | tf_op jit(solution)/shard_map/convert_element_type | solution.py:43
  162.3 3.8 %fusion.12 = bf16[1,384,2048]{1,2,0:T(8,128)(2,1)} fusion(bf16[1,384,2048]{1,2,0:T(8,128)(2,1)} %copy.22, f32[1,384,4,512]{1,3,2,0:T(8,128)S(1)} %copy.29), kind=kLoop, calls=%fused_computation.22 | loop fusion | flops 8650752 | bytes 6291456 | tf_op jit(solution)/shard_map/convert_element_type | solution.py:44
  166.0 2.6 %copy.30 = bf16[1,384,2048]{2,1,0:T(8,128)(2,1)} copy(bf16[1,384,2048]{1,2,0:T(8,128)(2,1)} %fusion.12) | data formatting | bytes 3145728 | tf_op jit(solution)/shard_map/convert_element_type | solution.py:44
  (5 shorter events, 0.0 us)
Async XLA Ops:
  6.5 1.4 copy-start.1
  6.5 2.3 %copy-start.4 = (bf16[2048]{0:T(1024)(128)(2,1)S(1)}, bf16[2048]{0:T(1024)(128)(2,1)}, u32[]{:S(2)}) copy-start(bf16[2048]{0:T(1024)(128)(2,1)} %param.8) | copy-start | bytes 12292
  6.5 2.3 %copy-start.5 = (bf16[2048]{0:T(1024)(128)(2,1)S(1)}, bf16[2048]{0:T(1024)(128)(2,1)}, u32[]{:S(2)}) copy-start(bf16[2048]{0:T(1024)(128)(2,1)} %param.9) | copy-start | bytes 12292
  6.5 63.4 %all-gather.2.cloned.1.call-start = ((), (), s32[]{:S(2)}) async-start(), calls=%async_computation.2 | async-start | bytes 10485760 | tf_op jit(solution)/shard_map/all_gather | solution.py:16
  13.3 8.3 %copy-start.3 = (bf16[4,1024]{1,0:T(4,128)(2,1)S(1)}, bf16[4,1024]{1,0:T(4,128)(2,1)}, u32[]{:S(2)}) copy-start(bf16[4,1024]{1,0:T(4,128)(2,1)} %param.11) | copy-start | bytes 24580
  15.0 43.3 %all-to-all-start = ((bf16[4,1,384,512]{3,2,1,0:T(8,128)(2,1)}), bf16[4,1,384,512]{3,2,1,0:T(8,128)(2,1)S(1)}, u32[]{:S(2)}, u32[]{:S(2)}) async-start(bf16[4,1,384,512]{3,2,1,0:T(8,128)(2,1)} %copy.24), calls=%async_computation | async-start | bytes 3145728 | tf_op jit(solution)/shard_map/all_to_all | solution.py:38
  58.3 1.1 copy-start
  83.4 1.4 slice-start
  108.0 8.8 %copy-start.2 = (bf16[1,384,2048]{2,1,0:T(8,128)(2,1)S(1)}, bf16[1,384,2048]{2,1,0:T(8,128)(2,1)}, u32[]{:S(2)}) copy-start(bf16[1,384,2048]{2,1,0:T(8,128)(2,1)} %param.6) | copy-start | bytes 4718596
  112.2 42.1 %all-to-all-start.1 = ((bf16[4,2,98304]{2,1,0:T(2,128)(2,1)}), bf16[4,2,98304]{2,1,0:T(2,128)(2,1)}, u32[]{:S(2)}, u32[]{:S(2)}) async-start(bf16[4,2,98304]{2,1,0:T(2,128)(2,1)} %reshape.73), calls=%async_computation.1 | async-start | bytes 3145728 | tf_op jit(solution)/shard_map/all_to_all | solution.py:42
Sparse Core Ops, SparseCore 0:
  8.9 60.9 all-gather.1
